TPU v7x, 32 devices: a whole 2x2x4 slice. The times are simulated.
32 devices in a mesh: sp: 4 (over z), fs: 4 (over y, x), tp: 2 (over core).
Axes of the slice: x: 2, y: 2, z: 4, core: 2. Of those that a mesh axis runs over, the one named last changes fastest.
Arguments:
- tokens: bfloat16 [4, 1024, 2048], P('fs', ('sp', 'tp')), may hold values from -6 to 6
- query_weight: bfloat16 [2048, 2048], P(('sp', 'fs'), 'tp'), may hold values from -0.125 to 0.125
- forget_weight: bfloat16 [2048, 2048], P(('sp', 'fs'), 'tp'), may hold values from -0.125 to 0.125
- value_weight: bfloat16 [2048, 2048], P(('sp', 'fs'), 'tp'), may hold values from -0.125 to 0.125
- convolution_gate_weight: bfloat16 [2048, 1024], P(('sp', 'fs'), 'tp'), may hold values from -0.125 to 0.125
- convolution_multiplier_weight: bfloat16 [2048, 1024], P(('sp', 'fs'), 'tp'), may hold values from -0.125 to 0.125
- convolution_input_weight: bfloat16 [2048, 1024], P(('sp', 'fs'), 'tp'), may hold values from -0.125 to 0.125
- gate_headroom: float32 [2048], P('tp'), may hold values from 9.765625e-05 to 0.06
- added_log_rate: float32 [4, 16, 1024], P('fs', 'tp', 'sp'), may hold values from -1.6 to 0
- initial_state: float32 [4, 16, 128, 128], P('fs', 'tp'), may hold values from -0.5 to 0.5
- head_norm_gain: float32 [2048], P('tp'), may hold values from 0.1 to 1.9
- convolution_taps: float32 [3, 1024], P(None, 'tp'), may hold values from -3.5 to 3.5
- convolution_bias: float32 [1024], P('tp'), may hold values from -4 to 4
- recurrence_output_weight: bfloat16 [2048, 2048], P('tp', ('sp', 'fs')), may hold values from -0.109375 to 0.109375
- convolution_output_weight: bfloat16 [1024, 2048], P('tp', ('sp', 'fs')), may hold values from -0.109375 to 0.109375
Outputs:
- mixed: bfloat16 [4, 1024, 2048], P('fs', ('sp', 'tp'))
All inputs are finite; a program needn't handle non-finite values.
Results may differ from a plain program's by a relative error of at most 0.018.
Values may be sent and summed in bfloat16 or wider, within the bound.
A program may use at most 64 MiB of HBM per device.

v0:
```python
import jax
import jax.numpy as jnp
from jax import lax
from jax.sharding import PartitionSpec as P

DK = 128
KW = 3
BLOCK_POSITIONS = 64


def carried_in(part, axis, combine, identity):
    place = lax.axis_index(axis)
    gathered = jax.tree.map(lambda a: lax.all_gather(a, axis), part)
    state = jax.tree.map(lambda a, e: jnp.zeros_like(a) + jnp.asarray(e, a.dtype), part, identity)

    def one(hop, state):
        return combine(
            state, jax.tree.map(lambda a: lax.dynamic_index_in_dim(a, hop, 0, False), gathered)
        )

    return lax.fori_loop(0, place, one, state)


def from_behind(block, axis, distance):
    devices = range(lax.axis_size(axis))
    route = [(i - distance, i) for i in devices if i - distance in devices]
    return lax.ppermute(block, axis, route)


def to_blocks(values, number_of_heads):
    number_of_blocks = values.shape[0] // BLOCK_POSITIONS
    return jnp.transpose(
        values.reshape(number_of_blocks, BLOCK_POSITIONS, number_of_heads, DK), (2, 0, 1, 3)
    )


def within_block_recurrence(
    query_vectors, forget_logits, value_vectors, gate_headroom, extra_rates
):
    number_of_heads = extra_rates.shape[0]
    number_of_blocks = query_vectors.shape[0] // BLOCK_POSITIONS
    query_scaled = to_blocks(query_vectors.astype(jnp.float32), number_of_heads) * DK ** (-0.5)
    gated_key = to_blocks(
        gate_headroom[None, :] * jax.nn.sigmoid(-forget_logits.astype(jnp.float32)), number_of_heads
    )
    forget_log_rate = (
        jnp.log1p(-gated_key)
        + extra_rates.reshape(number_of_heads, number_of_blocks, BLOCK_POSITIONS)[..., None]
    )
    values = to_blocks(value_vectors.astype(jnp.float32), number_of_heads)
    cumulative = jnp.cumsum(forget_log_rate, axis=2)
    query_decayed = query_scaled * jnp.exp(cumulative)
    key_decayed = gated_key * jnp.exp(-cumulative)
    scores = jnp.einsum(
        "hnik,hnjk->hnij", query_decayed, key_decayed, precision=lax.Precision.HIGHEST
    )
    causal = jnp.tril(jnp.ones((BLOCK_POSITIONS, BLOCK_POSITIONS), dtype=bool))
    scores = jnp.where(causal, scores, 0.0)
    within = jnp.einsum("hnij,hnjv->hniv", scores, values, precision=lax.Precision.HIGHEST)
    final_log = cumulative[:, :, -1, :]
    contrib = jnp.einsum(
        "hnck,hncv->hnkv",
        gated_key * jnp.exp(final_log[:, :, None, :] - cumulative),
        values,
        precision=lax.Precision.HIGHEST,
    )
    decays = jnp.exp(final_log)

    def advance(current, block_pair):
        return (block_pair[0][..., None] * current + block_pair[1], current)

    empty_state = jnp.zeros((number_of_heads, DK, DK), jnp.float32)
    local_total, entering = lax.scan(
        advance, empty_state, (jnp.moveaxis(decays, 1, 0), jnp.moveaxis(contrib, 1, 0))
    )
    entering = jnp.moveaxis(entering, 0, 1)
    before = jnp.exp(jnp.cumsum(final_log, axis=1) - final_log)
    device_decay = jnp.exp(jnp.sum(final_log, axis=1))
    return (query_decayed, within, entering, before, device_decay, local_total)


def finish(query_decayed, within, entering, before, carried, head_norm_gain):
    number_of_heads = query_decayed.shape[0]
    states = entering + before[..., None] * carried[:, None]
    carried_term = jnp.einsum(
        "hnck,hnkv->hncv", query_decayed, states, precision=lax.Precision.HIGHEST
    )
    length = query_decayed.shape[1] * BLOCK_POSITIONS
    recurrence_unnormed = jnp.transpose(within + carried_term, (1, 2, 0, 3)).reshape(
        length, number_of_heads, DK
    )
    mean_square = jnp.mean(recurrence_unnormed * recurrence_unnormed, axis=-1, keepdims=True)
    rec_out = (
        recurrence_unnormed
        * lax.rsqrt(mean_square + 1e-06)
        * head_norm_gain.reshape(number_of_heads, DK)
    )
    return rec_out.reshape(length, number_of_heads * DK).astype(jnp.bfloat16)


def chain_combine(earlier_part, later_part):
    return (
        earlier_part[0] * later_part[0],
        later_part[0][..., None] * earlier_part[1] + later_part[1],
    )


def shards(
    tokens,
    query_weight,
    forget_weight,
    value_weight,
    convolution_gate_weight,
    convolution_multiplier_weight,
    convolution_input_weight,
    gate_headroom,
    added_log_rate,
    initial_state,
    head_norm_gain,
    convolution_taps,
    convolution_bias,
    recurrence_output_weight,
    convolution_output_weight,
):
    own_rows = tokens[0]
    gathered = (
        lax.all_gather(query_weight, ("sp", "fs"), axis=0, tiled=True),
        lax.all_gather(forget_weight, ("sp", "fs"), axis=0, tiled=True),
        lax.all_gather(value_weight, ("sp", "fs"), axis=0, tiled=True),
        lax.all_gather(convolution_gate_weight, ("sp", "fs"), axis=0, tiled=True),
        lax.all_gather(convolution_multiplier_weight, ("sp", "fs"), axis=0, tiled=True),
        lax.all_gather(convolution_input_weight, ("sp", "fs"), axis=0, tiled=True),
        lax.all_gather(recurrence_output_weight, ("sp", "fs"), axis=1, tiled=True),
        lax.all_gather(convolution_output_weight, ("sp", "fs"), axis=1, tiled=True),
    )
    in_weights = gathered[:6]
    out_rec = gathered[6]
    out_conv = gathered[7]
    block_rows = lax.all_gather(own_rows, "tp", axis=0, tiled=True)
    projected = jnp.concatenate(
        [
            jnp.dot(block_rows, weight, preferred_element_type=jnp.float32).astype(jnp.bfloat16)
            for weight in in_weights
        ],
        axis=1,
    )
    rec_width = query_weight.shape[1]
    conv_width = convolution_gate_weight.shape[1]
    query_vectors = projected[:, :rec_width]
    forget_logits = projected[:, rec_width : 2 * rec_width]
    value_vectors = projected[:, 2 * rec_width : 3 * rec_width]
    conv_base = 3 * rec_width
    conv_gate = projected[:, conv_base : conv_base + conv_width]
    conv_mult = projected[:, conv_base + conv_width : conv_base + 2 * conv_width]
    conv_input = projected[:, conv_base + 2 * conv_width : conv_base + 3 * conv_width]
    query_decayed, within, entering, before, device_decay, local_total = within_block_recurrence(
        query_vectors, forget_logits, value_vectors, gate_headroom, added_log_rate[0]
    )
    conv_prod = conv_mult.astype(jnp.float32) * conv_input.astype(jnp.float32)
    length = conv_prod.shape[0]
    tail_rows = conv_prod[length - (KW - 1) :]
    unit_decay = jnp.ones_like(device_decay)
    empty_state = jnp.zeros_like(local_total)
    prior_decay, prior_state = carried_in(
        (device_decay, local_total), "sp", chain_combine, (unit_decay, empty_state)
    )
    prior_rows = from_behind(tail_rows, "sp", 1)
    carried = prior_decay[..., None] * initial_state[0] + prior_state
    rec_out = finish(query_decayed, within, entering, before, carried, head_norm_gain)
    extended = jnp.concatenate([prior_rows, conv_prod], axis=0)
    conv_y = jnp.broadcast_to(convolution_bias[None, :], conv_prod.shape)
    for j in range(KW):
        conv_y = conv_y + convolution_taps[j][None, :] * extended[j : j + length]
    conv_out = (conv_gate.astype(jnp.float32) * conv_y).astype(jnp.bfloat16)
    mixed = lax.psum_scatter(
        (
            jnp.dot(rec_out, out_rec, preferred_element_type=jnp.float32)
            + jnp.dot(conv_out, out_conv, preferred_element_type=jnp.float32)
        ).astype(jnp.bfloat16),
        "tp",
        scatter_dimension=0,
        tiled=True,
    )
    return mixed[None]


def solution(mesh):
    in_specs = (
        P("fs", ("sp", "tp"), None),
        P(("sp", "fs"), "tp"),
        P(("sp", "fs"), "tp"),
        P(("sp", "fs"), "tp"),
        P(("sp", "fs"), "tp"),
        P(("sp", "fs"), "tp"),
        P(("sp", "fs"), "tp"),
        P("tp"),
        P("fs", "tp", "sp"),
        P("fs", "tp", None, None),
        P("tp"),
        P(None, "tp"),
        P("tp"),
        P("tp", ("sp", "fs")),
        P("tp", ("sp", "fs")),
    )
    out_specs = P("fs", ("sp", "tp"), None)
    return jax.shard_map(shards, mesh=mesh, in_specs=in_specs, out_specs=out_specs, check_vma=False)
```

profile of v0, /device:TPU:0, one launch (start us, length us, event | category | flops | bytes accessed | tf_op | source)
XLA Modules:
  0.0 658.4 jit_solution(4386405157501010555)
XLA Ops:
  6.5 0.7 all-gather.30.cloned.1.call-update
  7.3 0.7 all-gather.14.cloned.1.call-update
  8.0 0.0 all-gather.16.cloned.1.call-start
  8.1 0.7 all-gather.16.cloned.1.call-update
  8.7 0.0 all-gather.18.cloned.1.call-start
  8.8 0.5 all-gather.18.cloned.1.call-update
  9.3 0.0 all-gather.26.cloned.1.call-start
  9.4 0.5 all-gather.26.cloned.1.call-update
  9.9 0.0 all-gather.24.cloned.1.call-start
  9.9 0.5 all-gather.24.cloned.1.call-update
  10.5 0.0 all-gather.32.cloned.1.call-start
  10.5 0.8 add.71
  11.3 0.1 copy.35
  11.5 9.2 %all-gather.30.cloned.1.call-done = bf16[1,256,2048]{2,1,0:T(8,128)(2,1)} async-done(((bf16[1,128,2048]{2,1,0:T(8,128)(2,1)}), bf16[1,256,2048]{2,1,0:T(8,128)(2,1)}) %all-gather.30.cloned.1.call-update) | async-done | bytes 1048592 | tf_op jit(solution)/shard_map/all_gather | solution.py:139
  20.7 79.6 %all-gather.14.cloned.1.call-done = bf16[2048,1024]{1,0:T(8,128)(2,1)} async-done(((bf16[128,1024]{1,0:T(8,128)(2,1)}), bf16[2048,1024]{1,0:T(8,128)(2,1)}) %all-gather.14.cloned.1.call-update) | async-done | bytes 4194320 | tf_op jit(solution)/shard_map/all_gather | solution.py:127
  100.2 3.8 fusion.17
  104.0 73.2 %all-gather.16.cloned.1.call-done = bf16[2048,1024]{1,0:T(8,128)(2,1)} async-done(((bf16[128,1024]{1,0:T(8,128)(2,1)}), bf16[2048,1024]{1,0:T(8,128)(2,1)}) %all-gather.16.cloned.1.call-update) | async-done | bytes 4194320 | tf_op jit(solution)/shard_map/all_gather | solution.py:128
  177.2 4.5 fusion.14
  181.7 72.3 %all-gather.18.cloned.1.call-done = bf16[2048,1024]{1,0:T(8,128)(2,1)} async-done(((bf16[128,1024]{1,0:T(8,128)(2,1)}), bf16[2048,1024]{1,0:T(8,128)(2,1)}) %all-gather.18.cloned.1.call-update) | async-done | bytes 4194320 | tf_op jit(solution)/shard_map/all_gather | solution.py:129
  254.1 3.5 fusion.18
  257.6 0.2 copy.48
  257.8 0.2 copy.47
  258.0 0.1 copy.49
  258.1 0.7 fusion.28
  258.9 1.8 bitcast_multiply_fusion.1
  260.7 2.1 convolution_bitcast_fusion
  262.8 4.6 while.26
  262.8 0.8 bitcast_dynamic-update-slice_fusion.2
  263.6 0.3 bitcast_add_fusion.8
  264.0 0.9 bitcast_dynamic-update-slice_fusion.2
  264.8 0.3 bitcast_add_fusion.8
  265.1 0.8 bitcast_dynamic-update-slice_fusion.2
  266.0 0.3 bitcast_add_fusion.8
  266.3 0.8 bitcast_dynamic-update-slice_fusion.2
  267.1 0.3 bitcast_add_fusion.8
  267.4 0.8 copy-done
  268.2 0.0 all-gather.20.cloned.1.call-start
  268.3 0.7 all-gather.20.cloned.1.call-update
  269.0 0.0 all-gather.22.cloned.1.call-start
  269.0 0.7 all-gather.22.cloned.1.call-update
  269.8 0.5 all-gather.28.cloned.1.call-update
  270.3 0.0 reduce-scatter.2.cloned.1.call-start
  270.4 45.3 %all-gather.26.cloned.1.call-done = bf16[2048,512]{1,0:T(8,128)(2,1)} async-done(((bf16[128,512]{1,0:T(8,128)(2,1)}), bf16[2048,512]{1,0:T(8,128)(2,1)}) %all-gather.26.cloned.1.call-update) | async-done | bytes 2097168 | tf_op jit(solution)/shard_map/all_gather | solution.py:132
  315.7 2.6 fusion.22
  318.3 59.2 %all-gather.24.cloned.1.call-done = bf16[2048,512]{1,0:T(8,128)(2,1)} async-done(((bf16[128,512]{1,0:T(8,128)(2,1)}), bf16[2048,512]{1,0:T(8,128)(2,1)}) %all-gather.24.cloned.1.call-update) | async-done | bytes 2097168 | tf_op jit(solution)/shard_map/all_gather | solution.py:131
  377.5 2.4 fusion.21
  380.0 3.4 collective-permute-start
  383.3 13.9 %all-gather.1 = f32[32,128]{1,0:T(8,128)S(1)} all-gather(f32[8,128]{1,0:T(8,128)S(1)} %exp.41), channel_id=3, replica_groups=mesh['sp'=4,'fs'=4,'tp'=2] {'sp'}, dimensions={0}, use_global_device_ids=true | all-gather | bytes 20480 | tf_op jit(solution)/shard_map/all_gather | solution.py:13
  397.2 0.8 fusion.23
  398.1 2.9 convolution_select_fusion
  401.0 0.7 fusion.53
  401.7 22.1 %all-gather.32.cloned.1.call-done = f32[32,128,128]{2,1,0:T(8,128)} async-done(((f32[8,128,128]{2,1,0:T(8,128)}), f32[32,128,128]{2,1,0:T(8,128)}) %all-gather.32.cloned.1.call-update) | async-done | bytes 2097168 | tf_op jit(solution)/shard_map/all_gather | solution.py:13
  423.8 1.0 copy-done.8
  424.8 0.2 fusion.51
  425.0 5.1 multiply_reduce_fusion
  430.2 0.1 copy.45
  430.3 1.8 copy.43
  432.1 81.8 %all-gather.20.cloned.1.call-done = bf16[1024,2048]{1,0:T(8,128)(2,1)} async-done(((bf16[1024,128]{1,0:T(8,128)(2,1)}), bf16[1024,2048]{1,0:T(8,128)(2,1)}) %all-gather.20.cloned.1.call-update) | async-done | bytes 4194320 | tf_op jit(solution)/shard_map/all_gather | solution.py:133
  514.0 0.3 mul.146
  514.3 3.6 fusion.48
  517.9 57.4 %all-gather.22.cloned.1.call-done = bf16[2048,512]{1,0:T(8,128)(2,1)} async-done(((bf16[128,512]{1,0:T(8,128)(2,1)}), bf16[2048,512]{1,0:T(8,128)(2,1)}) %all-gather.22.cloned.1.call-update) | async-done | bytes 2097168 | tf_op jit(solution)/shard_map/all_gather | solution.py:130
  575.3 64.3 %all-gather.28.cloned.1.call-done = bf16[512,2048]{1,0:T(8,128)(2,1)} async-done(((bf16[512,128]{1,0:T(8,128)(2,1)}), bf16[512,2048]{1,0:T(8,128)(2,1)}) %all-gather.28.cloned.1.call-update) | async-done | bytes 2097168 | tf_op jit(solution)/shard_map/all_gather | solution.py:134
  639.7 5.5 fusion
  645.1 6.7 %reduce-scatter.2.cloned.1.call-done = bf16[128,2048]{1,0:T(8,128)(2,1)} async-done(((bf16[256,2048]{1,0:T(8,128)(2,1)}), bf16[128,2048]{1,0:T(8,128)(2,1)}) %reduce-scatter.2.cloned.1.call-update) | async-done | bytes 524304 | tf_op jit(solution)/shard_map/reduce_scatter | solution.py:175
  (46 shorter events, 0.3 us)
Async XLA Ops:
  6.5 14.1 %all-gather.30.cloned.1.call-start = ((), (), s32[]{:S(2)}) async-start(), calls=%async_computation.10 | async-start | bytes 1572864 | tf_op jit(solution)/shard_map/all_gather | solution.py:139
  7.3 93.0 %all-gather.14.cloned.1.call-start = ((), (), s32[]{:S(2)}) async-start(), calls=%async_computation.1 | async-start | bytes 4456448 | tf_op jit(solution)/shard_map/all_gather | solution.py:127
  8.0 169.2 %all-gather.16.cloned.1.call-start = ((), (), s32[]{:S(2)}) async-start(), calls=%async_computation.2 | async-start | bytes 4456448 | tf_op jit(solution)/shard_map/all_gather | solution.py:128
  8.7 245.3 %all-gather.18.cloned.1.call-start = ((), (), s32[]{:S(2)}) async-start(), calls=%async_computation.3 | async-start | bytes 4456448 | tf_op jit(solution)/shard_map/all_gather | solution.py:129
  9.3 306.4 %all-gather.26.cloned.1.call-start = ((), (), s32[]{:S(2)}) async-start(), calls=%async_computation.7 | async-start | bytes 2228224 | tf_op jit(solution)/shard_map/all_gather | solution.py:132
  9.9 367.6 %all-gather.24.cloned.1.call-start = ((), (), s32[]{:S(2)}) async-start(), calls=%async_computation.6 | async-start | bytes 2228224 | tf_op jit(solution)/shard_map/all_gather | solution.py:131
  10.5 413.3 %all-gather.32.cloned.1.call-start = ((), (), s32[]{:S(2)}) async-start(), calls=%async_computation.11 | async-start | bytes 2621440 | tf_op jit(solution)/shard_map/all_gather | solution.py:13
  11.4 165.8 %copy-start.12 = (f32[1024]{0:T(1024)S(1)}, f32[1024]{0:T(1024)}, u32[]{:S(2)}) copy-start(f32[1024]{0:T(1024)} %param.26) | copy-start | bytes 12292
  20.7 156.6 %copy-start.3 = (bf16[1,256,2048]{2,1,0:T(8,128)(2,1)S(1)}, bf16[1,256,2048]{2,1,0:T(8,128)(2,1)}, u32[]{:S(2)}) copy-start(bf16[1,256,2048]{2,1,0:T(8,128)(2,1)} %all-gather.30.cloned.1.call-done) | copy-start | bytes 3145732
  254.1 3.5 copy-start.7
  258.8 1.8 copy-start.2
  262.8 7.6 %copy-start.10 = (f32[3,512]{1,0:T(4,128)S(1)}, f32[3,512]{1,0:T(4,128)}, u32[]{:S(2)}) copy-start(f32[3,512]{1,0:T(4,128)} %param.30) | copy-start | bytes 18436
  267.4 0.8 copy-start
  268.2 109.3 %copy-start.4 = (bf16[1,256,2048]{2,1,0:T(8,128)(2,1)S(1)}, bf16[1,256,2048]{2,1,0:T(8,128)(2,1)}, u32[]{:S(2)}) copy-start(bf16[1,256,2048]{2,1,0:T(8,128)(2,1)} %all-gather.30.cloned.1.call-done) | copy-start | bytes 3145732
  268.2 245.7 %all-gather.20.cloned.1.call-start = ((), (), s32[]{:S(2)}) async-start(), calls=%async_computation.4 | async-start | bytes 4456448 | tf_op jit(solution)/shard_map/all_gather | solution.py:133
  269.0 306.3 %all-gather.22.cloned.1.call-start = ((), (), s32[]{:S(2)}) async-start(), calls=%async_computation.5 | async-start | bytes 2228224 | tf_op jit(solution)/shard_map/all_gather | solution.py:130
  269.7 369.9 %all-gather.28.cloned.1.call-start = ((), (), s32[]{:S(2)}) async-start(), calls=%async_computation.8 | async-start | bytes 2228224 | tf_op jit(solution)/shard_map/all_gather | solution.py:134
  270.3 381.6 %reduce-scatter.2.cloned.1.call-start = ((), (), s32[]{:S(2)}) async-start(), calls=%async_computation.9 | async-start | bytes 1572864 | tf_op jit(solution)/shard_map/reduce_scatter | solution.py:175
  318.3 79.7 %copy-start.1 = (f32[8,4,64,128]{3,0,1,2:T(8,128)S(1)}, f32[8,4,64,128]{3,0,1,2:T(8,128)}, u32[]{:S(2)}) copy-start(f32[8,4,64,128]{3,0,1,2:T(8,128)} %get-tuple-element.132) | copy-start | bytes 3145732
  377.5 20.5 %copy-start.5 = (f32[8,4,64,128]{3,0,1,2:T(8,128)S(1)}, f32[8,4,64,128]{3,0,1,2:T(8,128)}, u32[]{:S(2)}) copy-start(f32[8,4,64,128]{3,0,1,2:T(8,128)} %get-tuple-element.129) | copy-start | bytes 3145732
  379.9 18.1 %copy-start.6 = (f32[256,512]{1,0:T(8,128)}, f32[256,512]{1,0:T(8,128)S(1)}, u32[]{:S(2)}) copy-start(f32[256,512]{1,0:T(8,128)S(1)} %fusion.21) | copy-start | bytes 1572868
  380.0 259.7 %collective-permute-start = (f32[2,512]{1,0:T(2,128)S(1)}, f32[2,512]{1,0:T(2,128)S(1)}, u32[]{:S(2)}, u32[]{:S(2)}) collective-permute-start(f32[2,512]{1,0:T(2,128)S(1)} %slice.29), channel_id=1, source_target_pairs={{0,8},{8,16},{16,24},{1,9},{9,17},{17,25},{2,10},{10,18},{18,26},{... | collective-permute-start | bytes 12296 | tf_op jit(solution)/shard_map/ppermute | solution.py:27
  423.8 1.0 copy-start.8
  430.2 84.1 %copy-start.9 = (f32[1024]{0:T(1024)S(1)}, f32[1024]{0:T(1024)}, u32[]{:S(2)}) copy-start(f32[1024]{0:T(1024)} %param.29) | copy-start | bytes 12292
  514.3 125.4 %copy-start.11 = (f32[512]{0:T(512)S(1)}, f32[512]{0:T(512)}, u32[]{:S(2)}) copy-start(f32[512]{0:T(512)} %param.31) | copy-start | bytes 6148
Sparse Core Ops, SparseCore 0:
  8.9 11.7 all-gather.29
  23.4 76.7 all-gather.13
  103.0 74.1 all-gather.15
  179.8 74.1 all-gather.17
  256.7 58.9 all-gather.25
  318.3 59.1 all-gather.23
  379.1 44.5 all-gather.31
  426.4 87.4 all-gather.19
  516.7 58.5 all-gather.21
  577.9 61.7 all-gather.27
  645.3 6.5 reduce-scatter.1
where the time goes:
time: 659 us; the launch traced here: 658 us
  waiting for transfers between devices  577 us (88%)
  matrix products  36.7 us (6%)
  blocking collectives  13.9 us (2%)
  between operations  13.6 us (2%)
  other arithmetic  8.04 us (1%)
    all_gather x1, waiting for transfers between devices, shards(): lax.all_gather(recurrence_output_weight, ('sp', 'fs'), axis=1, tiled=True)  81.8 us
    all_gather x1, waiting for transfers between devices, shards(): lax.all_gather(query_weight, ('sp', 'fs'), axis=0, tiled=True)  79.6 us
    all_gather x1, waiting for transfers between devices, shards(): lax.all_gather(forget_weight, ('sp', 'fs'), axis=0, tiled=True)  73.2 us
    all_gather x1, waiting for transfers between devices, shards(): lax.all_gather(value_weight, ('sp', 'fs'), axis=0, tiled=True)  72.3 us
    all_gather x1, waiting for transfers between devices, shards(): lax.all_gather(convolution_output_weight, ('sp', 'fs'), axis=1, tiled=True)  64.3 us
    all_gather x1, waiting for transfers between devices, shards(): lax.all_gather(convolution_multiplier_weight, ('sp', 'fs'), axis=0, tiled...  59.2 us
    all_gather x1, waiting for transfers between devices, shards(): lax.all_gather(convolution_gate_weight, ('sp', 'fs'), axis=0, tiled=True)  57.4 us
    all_gather x1, waiting for transfers between devices, shards(): lax.all_gather(convolution_input_weight, ('sp', 'fs'), axis=0, tiled=True)  45.3 us
  transfers between devices with their start and end apart: 12, of which 11 were waited for; matrix products, arithmetic and copies ran while one was open for 7% of the time, Pallas kernels for 0%

commit v1 on v0

--- a/solution.py
+++ b/solution.py
@@ -130,7 +130,7 @@
         lax.all_gather(convolution_gate_weight, ("sp", "fs"), axis=0, tiled=True),
         lax.all_gather(convolution_multiplier_weight, ("sp", "fs"), axis=0, tiled=True),
         lax.all_gather(convolution_input_weight, ("sp", "fs"), axis=0, tiled=True),
-        lax.all_gather(recurrence_output_weight, ("sp", "fs"), axis=1, tiled=True),
+        jnp.concatenate(lax.all_gather(recurrence_output_weight, ("sp", "fs")), axis=1),
         lax.all_gather(convolution_output_weight, ("sp", "fs"), axis=1, tiled=True),
     )
     in_weights = gathered[:6]

time: 659 us -> 646 us (0.980)
  waiting for transfers between devices: 577 us -> 559 us
    all_gather x1, waiting for transfers between devices: 81.8 us -> 58.1 us  [shards(): lax.all_gather(recurrence_output_weight, ('sp', 'fs'))]
    all_gather x1, waiting for transfers between devices: 22.1 us -> 32.8 us  [carried_in(): gathered = jax.tree.map(lambda a: lax.all_gather(a, axis), part)]
    all_gather x1, waiting for transfers between devices: 79.6 us -> 73 us  [shards(): lax.all_gather(query_weight, ('sp', 'fs'), axis=0, tiled=True)]
  transfers between devices with their start and end apart: 12 -> 12, of which waited for: 11 -> 11; matrix products, arithmetic and copies ran while one was open for 7% -> 8% of each run, Pallas kernels for 0% -> 0%
where the time goes in v1:
time: 646 us; the launch traced here: 645 us
  waiting for transfers between devices  559 us (87%)
  matrix products  35.8 us (6%)
  between operations  13.5 us (2%)
  blocking collectives  13.4 us (2%)
  local copies, waits for them, and re-layouts  10.5 us (2%)
  other arithmetic  9.54 us (1%)
    all_gather x1, waiting for transfers between devices, shards(): lax.all_gather(forget_weight, ('sp', 'fs'), axis=0, tiled=True)  79.6 us
    all_gather x1, waiting for transfers between devices, shards(): lax.all_gather(query_weight, ('sp', 'fs'), axis=0, tiled=True)  73 us
    all_gather x1, waiting for transfers between devices, shards(): lax.all_gather(value_weight, ('sp', 'fs'), axis=0, tiled=True)  72.2 us
    all_gather x1, waiting for transfers between devices, shards(): lax.all_gather(convolution_output_weight, ('sp', 'fs'), axis=1, tiled=True)  64.3 us
    all_gather x1, waiting for transfers between devices, shards(): lax.all_gather(convolution_multiplier_weight, ('sp', 'fs'), axis=0, tiled...  59.2 us
    all_gather x1, waiting for transfers between devices, shards(): lax.all_gather(recurrence_output_weight, ('sp', 'fs'))  58.1 us
    all_gather x1, waiting for transfers between devices, shards(): lax.all_gather(convolution_gate_weight, ('sp', 'fs'), axis=0, tiled=True)  52.7 us
    all_gather x1, waiting for transfers between devices, shards(): lax.all_gather(convolution_input_weight, ('sp', 'fs'), axis=0, tiled=True)  46.2 us
  transfers between devices with their start and end apart: 12, of which 11 were waited for; matrix products, arithmetic and copies ran while one was open for 8% of the time, Pallas kernels for 0%

profile of v1, /device:TPU:0, one launch (start us, length us, event | category | flops | bytes accessed | tf_op | source)
XLA Modules:
  0.0 645.4 jit_solution(3989105264493336645)
XLA Ops:
  6.5 0.7 all-gather.29.cloned.1.call-update
  7.3 0.7 all-gather.17.cloned.1.call-update
  8.0 0.0 all-gather.15.cloned.1.call-start
  8.1 0.7 all-gather.15.cloned.1.call-update
  8.7 0.0 all-gather.19.cloned.1.call-start
  8.8 0.5 all-gather.19.cloned.1.call-update
  9.3 0.0 all-gather.25.cloned.1.call-start
  9.4 0.5 all-gather.25.cloned.1.call-update
  9.9 0.0 all-gather.23.cloned.1.call-start
  9.9 0.5 all-gather.23.cloned.1.call-update
  10.5 0.7 all-gather.33.cloned.1.call-update
  11.2 0.0 all-gather.31.cloned.1.call-start
  11.3 0.8 add.70
  12.1 0.1 copy.47
  12.2 8.5 %all-gather.29.cloned.1.call-done = bf16[1,256,2048]{2,1,0:T(8,128)(2,1)} async-done(((bf16[1,128,2048]{2,1,0:T(8,128)(2,1)}), bf16[1,256,2048]{2,1,0:T(8,128)(2,1)}) %all-gather.29.cloned.1.call-update) | async-done | bytes 1048592 | tf_op jit(solution)/shard_map/all_gather | solution.py:139
  20.7 79.6 %all-gather.17.cloned.1.call-done = bf16[2048,1024]{1,0:T(8,128)(2,1)} async-done(((bf16[128,1024]{1,0:T(8,128)(2,1)}), bf16[2048,1024]{1,0:T(8,128)(2,1)}) %all-gather.17.cloned.1.call-update) | async-done | bytes 4194320 | tf_op jit(solution)/shard_map/all_gather | solution.py:128
  100.2 3.8 fusion.14
  104.1 0.2 copy.59
  104.3 73.0 %all-gather.15.cloned.1.call-done = bf16[2048,1024]{1,0:T(8,128)(2,1)} async-done(((bf16[128,1024]{1,0:T(8,128)(2,1)}), bf16[2048,1024]{1,0:T(8,128)(2,1)}) %all-gather.15.cloned.1.call-update) | async-done | bytes 4194320 | tf_op jit(solution)/shard_map/all_gather | solution.py:127
  177.2 3.4 fusion.17
  180.7 1.2 copy.58
  181.8 72.2 %all-gather.19.cloned.1.call-done = bf16[2048,1024]{1,0:T(8,128)(2,1)} async-done(((bf16[128,1024]{1,0:T(8,128)(2,1)}), bf16[2048,1024]{1,0:T(8,128)(2,1)}) %all-gather.19.cloned.1.call-update) | async-done | bytes 4194320 | tf_op jit(solution)/shard_map/all_gather | solution.py:129
  254.1 3.4 fusion.18
  257.5 0.1 copy.60
  257.6 0.7 fusion.26
  258.4 0.4 copy-done.7
  258.7 1.8 bitcast_multiply_fusion
  260.5 2.1 convolution_bitcast_fusion
  262.7 4.6 while.26
  262.7 0.8 bitcast_dynamic-update-slice_fusion.2
  263.5 0.3 bitcast_add_fusion.8
  263.8 0.8 bitcast_dynamic-update-slice_fusion.2
  264.7 0.3 bitcast_add_fusion.8
  265.0 0.8 bitcast_dynamic-update-slice_fusion.2
  265.8 0.3 bitcast_add_fusion.8
  266.2 0.8 bitcast_dynamic-update-slice_fusion.2
  267.0 0.3 bitcast_add_fusion.8
  267.3 0.8 copy-done
  268.1 0.0 all-gather.21.cloned.1.call-start
  268.2 0.7 all-gather.21.cloned.1.call-update
  268.9 0.5 all-gather.27.cloned.1.call-update
  269.5 0.0 reduce-scatter.2.cloned.1.call-start
  269.5 46.2 %all-gather.25.cloned.1.call-done = bf16[2048,512]{1,0:T(8,128)(2,1)} async-done(((bf16[128,512]{1,0:T(8,128)(2,1)}), bf16[2048,512]{1,0:T(8,128)(2,1)}) %all-gather.25.cloned.1.call-update) | async-done | bytes 2097168 | tf_op jit(solution)/shard_map/all_gather | solution.py:132
  315.7 2.6 fusion.22
  318.3 59.2 %all-gather.23.cloned.1.call-done = bf16[2048,512]{1,0:T(8,128)(2,1)} async-done(((bf16[128,512]{1,0:T(8,128)(2,1)}), bf16[2048,512]{1,0:T(8,128)(2,1)}) %all-gather.23.cloned.1.call-update) | async-done | bytes 2097168 | tf_op jit(solution)/shard_map/all_gather | solution.py:131
  377.5 2.3 fusion.21
  379.9 3.4 collective-permute-start
  383.2 13.4 %all-gather.1 = f32[32,128]{1,0:T(8,128)S(1)} all-gather(f32[8,128]{1,0:T(8,128)S(1)} %exp.41), channel_id=3, replica_groups=mesh['sp'=4,'fs'=4,'tp'=2] {'sp'}, dimensions={0}, use_global_device_ids=true | all-gather | bytes 20480 | tf_op jit(solution)/shard_map/all_gather | solution.py:13
  396.6 58.1 %all-gather.33.cloned.1.call-done = bf16[16384,128]{1,0:T(8,128)(2,1)} async-done(((bf16[1024,128]{1,0:T(8,128)(2,1)}), bf16[16384,128]{1,0:T(8,128)(2,1)}) %all-gather.33.cloned.1.call-update) | async-done | bytes 4194320 | tf_op jit(solution)/shard_map/all_gather | solution.py:133
  454.7 6.5 %copy.56 = bf16[1024,16,128]{0,2,1:T(8,128)(2,1)} copy(bf16[1024,16,128]{2,0,1:T(8,128)(2,1)} %bitcast.128) | data formatting | bytes 8388608 | tf_op jit(solution)/shard_map/reshape | solution.py:133
  461.2 4.1 convolution_select_fusion
  465.3 0.8 fusion.23
  466.2 1.6 fusion.52
  467.8 32.8 %all-gather.31.cloned.1.call-done = f32[32,128,128]{2,1,0:T(8,128)} async-done(((f32[8,128,128]{2,1,0:T(8,128)}), f32[32,128,128]{2,1,0:T(8,128)}) %all-gather.31.cloned.1.call-update) | async-done | bytes 2097168 | tf_op jit(solution)/shard_map/all_gather | solution.py:13
  500.6 1.3 fusion.50
  502.0 0.0 copy-done.6
  502.0 4.4 multiply_reduce_fusion
  506.5 0.3 multiply_convert_fusion
  506.8 0.3 copy.55
  507.2 2.7 fusion.46
  509.8 52.7 %all-gather.21.cloned.1.call-done = bf16[2048,512]{1,0:T(8,128)(2,1)} async-done(((bf16[128,512]{1,0:T(8,128)(2,1)}), bf16[2048,512]{1,0:T(8,128)(2,1)}) %all-gather.21.cloned.1.call-update) | async-done | bytes 2097168 | tf_op jit(solution)/shard_map/all_gather | solution.py:130
  562.6 64.3 %all-gather.27.cloned.1.call-done = bf16[512,2048]{1,0:T(8,128)(2,1)} async-done(((bf16[512,128]{1,0:T(8,128)(2,1)}), bf16[512,2048]{1,0:T(8,128)(2,1)}) %all-gather.27.cloned.1.call-update) | async-done | bytes 2097168 | tf_op jit(solution)/shard_map/all_gather | solution.py:134
  626.9 5.3 fusion
  632.2 6.7 %reduce-scatter.2.cloned.1.call-done = bf16[128,2048]{1,0:T(8,128)(2,1)} async-done(((bf16[256,2048]{1,0:T(8,128)(2,1)}), bf16[128,2048]{1,0:T(8,128)(2,1)}) %reduce-scatter.2.cloned.1.call-update) | async-done | bytes 524304 | tf_op jit(solution)/shard_map/reduce_scatter | solution.py:175
  (42 shorter events, 0.3 us)
Async XLA Ops:
  6.5 14.1 %all-gather.29.cloned.1.call-start = ((), (), s32[]{:S(2)}) async-start(), calls=%async_computation.9 | async-start | bytes 1572864 | tf_op jit(solution)/shard_map/all_gather | solution.py:139
  7.3 93.0 %all-gather.17.cloned.1.call-start = ((), (), s32[]{:S(2)}) async-start(), calls=%async_computation.2 | async-start | bytes 4456448 | tf_op jit(solution)/shard_map/all_gather | solution.py:128
  8.0 169.2 %all-gather.15.cloned.1.call-start = ((), (), s32[]{:S(2)}) async-start(), calls=%async_computation.1 | async-start | bytes 4456448 | tf_op jit(solution)/shard_map/all_gather | solution.py:127
  8.7 245.3 %all-gather.19.cloned.1.call-start = ((), (), s32[]{:S(2)}) async-start(), calls=%async_computation.3 | async-start | bytes 4456448 | tf_op jit(solution)/shard_map/all_gather | solution.py:129
  9.3 306.4 %all-gather.25.cloned.1.call-start = ((), (), s32[]{:S(2)}) async-start(), calls=%async_computation.6 | async-start | bytes 2228224 | tf_op jit(solution)/shard_map/all_gather | solution.py:132
  9.9 367.6 %all-gather.23.cloned.1.call-start = ((), (), s32[]{:S(2)}) async-start(), calls=%async_computation.5 | async-start | bytes 2228224 | tf_op jit(solution)/shard_map/all_gather | solution.py:131
  10.5 444.2 %all-gather.33.cloned.1.call-start = ((), (), s32[]{:S(2)}) async-start(), calls=%async_computation.11 | async-start | bytes 4456448 | tf_op jit(solution)/shard_map/all_gather | solution.py:133
  11.2 489.3 %all-gather.31.cloned.1.call-start = ((), (), s32[]{:S(2)}) async-start(), calls=%async_computation.10 | async-start | bytes 2621440 | tf_op jit(solution)/shard_map/all_gather | solution.py:13
  104.1 73.2 %copy-start.4 = (bf16[1,256,2048]{2,1,0:T(8,128)(2,1)S(1)}, bf16[1,256,2048]{2,1,0:T(8,128)(2,1)}, u32[]{:S(2)}) copy-start(bf16[1,256,2048]{2,1,0:T(8,128)(2,1)} %all-gather.29.cloned.1.call-done) | copy-start | bytes 3145732
  257.5 1.2 copy-start.7
  258.3 2.2 copy-start.2
  262.7 6.9 %copy-start.8 = (f32[3,512]{1,0:T(4,128)S(1)}, f32[3,512]{1,0:T(4,128)}, u32[]{:S(2)}) copy-start(f32[3,512]{1,0:T(4,128)} %param.30) | copy-start | bytes 18436
  267.3 0.8 copy-start
  268.1 109.4 %copy-start.5 = (bf16[1,256,2048]{2,1,0:T(8,128)(2,1)S(1)}, bf16[1,256,2048]{2,1,0:T(8,128)(2,1)}, u32[]{:S(2)}) copy-start(bf16[1,256,2048]{2,1,0:T(8,128)(2,1)} %all-gather.29.cloned.1.call-done) | copy-start | bytes 3145732
  268.1 294.4 %all-gather.21.cloned.1.call-start = ((), (), s32[]{:S(2)}) async-start(), calls=%async_computation.4 | async-start | bytes 2228224 | tf_op jit(solution)/shard_map/all_gather | solution.py:130
  268.9 358.0 %all-gather.27.cloned.1.call-start = ((), (), s32[]{:S(2)}) async-start(), calls=%async_computation.7 | async-start | bytes 2228224 | tf_op jit(solution)/shard_map/all_gather | solution.py:134
  269.5 369.4 %reduce-scatter.2.cloned.1.call-start = ((), (), s32[]{:S(2)}) async-start(), calls=%async_computation.8 | async-start | bytes 1572864 | tf_op jit(solution)/shard_map/reduce_scatter | solution.py:175
  379.9 247.0 %collective-permute-start = (f32[2,512]{1,0:T(2,128)S(1)}, f32[2,512]{1,0:T(2,128)S(1)}, u32[]{:S(2)}, u32[]{:S(2)}) collective-permute-start(f32[2,512]{1,0:T(2,128)S(1)} %slice.29), channel_id=1, source_target_pairs={{0,8},{8,16},{16,24},{1,9},{9,17},{17,25},{2,10},{10,18},{18,26},{... | collective-permute-start | bytes 12296 | tf_op jit(solution)/shard_map/ppermute | solution.py:27
  454.7 6.5 %copy-start.1 = (f32[8,4,64,128]{3,0,1,2:T(8,128)S(1)}, f32[8,4,64,128]{3,0,1,2:T(8,128)}, u32[]{:S(2)}) copy-start(f32[8,4,64,128]{3,0,1,2:T(8,128)} %get-tuple-element.137) | copy-start | bytes 3145732
  500.6 1.4 copy-start.6
  502.0 4.4 copy-start.9
  502.0 5.1 copy-start.3
  507.2 119.7 %copy-start.10 = (f32[512]{0:T(512)S(1)}, f32[512]{0:T(512)}, u32[]{:S(2)}) copy-start(f32[512]{0:T(512)} %param.31) | copy-start | bytes 6148
Sparse Core Ops, SparseCore 0:
  8.9 11.7 all-gather.28
  23.4 76.7 all-gather.16
  103.0 74.1 all-gather.14
  179.8 74.1 all-gather.18
  256.7 58.9 all-gather.24
  318.3 59.1 all-gather.22
  380.3 74.3 all-gather.32
  456.3 44.2 all-gather.30
  503.3 59.1 all-gather.20
  565.1 61.7 all-gather.26
  632.3 6.5 reduce-scatter.1
